TPU v7x, 32 devices: a whole 2x2x4 slice. The times are simulated.
32 devices in a mesh: sp: 8 (over z, x), tp: 4 (over y, core).
Axes of the slice: x: 2, y: 2, z: 4, core: 2. Of those that a mesh axis runs over, the one named last changes fastest.
Arguments:
- skip_stream_input: bfloat16 [1024, 2048], P('sp'), may hold values from -16 to 16
- asking_vectors_split: bfloat16 [1024, 2048], P('sp', 'tp'), may hold values from -8 to 8
- lookup_vectors_split: bfloat16 [1024, 512], P('sp'), may hold values from -8 to 8
- content_vectors_split: bfloat16 [1024, 512], P('sp'), may hold values from -6 to 6
- asking_rms_gain: float32 [128], replicated, may hold values from 0.1 to 1.9
- lookup_rms_gain: float32 [128], replicated, may hold values from 0.1 to 1.9
- softness_per_channel: float32 [16], P('tp'), may hold values from 1.5 to 24
- mixing_exit_weights: bfloat16 [2048, 2048], P('tp'), may hold values from -0.125 to 0.125
- specialist_rms_gain: float32 [2048], replicated, may hold values from 0.1 to 1.9
- selected_dispatch_weights: float32 [1024, 2], P('sp'), may hold values from -6 to 6
- selected_specialist_ids: int32 [1024, 2], P('sp'), may hold values from 0 to 7, all different within a row; in each aligned block of 128 rows (0 to 127, 128 to 255, ...) at most 48 rows name the same one
- specialist_switch_weights: bfloat16 [8, 2048, 2048], P('sp', None, 'tp'), may hold values from -0.125 to 0.125
- specialist_widen_weights: bfloat16 [8, 2048, 2048], P('sp', None, 'tp'), may hold values from -0.125 to 0.125
- specialist_shrink_weights: bfloat16 [8, 2048, 2048], P('sp', 'tp'), may hold values from -0.125 to 0.125
Outputs:
- layer_out: bfloat16 [1024, 2048], P('sp', 'tp')
Inputs may be any that keep to these rules, and one draw needn't show every extreme that they name: `selected_specialist_ids`: each row names 2 different experts. In each aligned block of 128 rows no expert is named by more than 48 rows, a bound that some block reaches.
All inputs are finite; a program needn't handle non-finite values.
Results may differ from a plain program's by a relative error of at most 0.0085.
Values may be sent and summed in bfloat16 or wider, within the bound.
A program may use at most 64 MiB of HBM per device.

v0:
```python
import math
import jax
import jax.numpy as jnp
from jax import lax
from jax.sharding import PartitionSpec as P

CHANNEL_WIDTH = 128
GROUP = 4
GRID_W = 64
EPSILON = 1e-06
NEGATIVE = -1e30


def rotate_half(values_in, positions, full_width):
    half_width = full_width // 2
    frequency = 10000.0 ** (-jnp.arange(half_width, dtype=jnp.float32) / half_width)
    angles = positions.astype(jnp.float32)[:, None] * frequency[None, :]
    cosine = jnp.cos(angles)[:, None, :]
    sine = jnp.sin(angles)[:, None, :]
    leading = values_in[..., :half_width]
    trailing = values_in[..., half_width:]
    return jnp.concatenate(
        [leading * cosine - trailing * sine, trailing * cosine + leading * sine], axis=-1
    )


def norm_rotate(heads_in, gain_vec, positions):
    widened = heads_in.astype(jnp.float32)
    scaled = (
        widened
        * lax.rsqrt(jnp.mean(widened * widened, axis=-1, keepdims=True) + EPSILON)
        * gain_vec
    )
    half_width = scaled.shape[-1] // 2
    grid_rows = positions // GRID_W
    grid_cols = positions % GRID_W
    turned = jnp.concatenate(
        [
            rotate_half(scaled[..., :half_width], grid_rows, half_width),
            rotate_half(scaled[..., half_width:], grid_cols, half_width),
        ],
        axis=-1,
    )
    return turned.astype(jnp.bfloat16)


def shards(
    skip_stream_input,
    asking_vectors_split,
    lookup_vectors_split,
    content_vectors_split,
    asking_rms_gain,
    lookup_rms_gain,
    softness_per_channel,
    mixing_exit_weights,
    specialist_rms_gain,
    selected_dispatch_weights,
    selected_specialist_ids,
    specialist_switch_weights,
    specialist_widen_weights,
    specialist_shrink_weights,
):
    tok_count = skip_stream_input.shape[0]
    model_width = skip_stream_input.shape[1]
    heads_here = asking_vectors_split.shape[1] // CHANNEL_WIDTH
    local_key_value_heads = max(1, heads_here // GROUP)
    local_group_count = heads_here // local_key_value_heads
    tp_position = lax.axis_index("tp")
    positions = lax.axis_index("sp") * tok_count + jnp.arange(tok_count, dtype=jnp.int32)
    query_turned = norm_rotate(
        asking_vectors_split.reshape(tok_count, heads_here, CHANNEL_WIDTH),
        asking_rms_gain,
        positions,
    )
    first_head = tp_position * heads_here // GROUP
    key_cols = lax.dynamic_slice_in_dim(
        lookup_vectors_split, first_head * CHANNEL_WIDTH, local_key_value_heads * CHANNEL_WIDTH, 1
    )
    value_cols = lax.dynamic_slice_in_dim(
        content_vectors_split, first_head * CHANNEL_WIDTH, local_key_value_heads * CHANNEL_WIDTH, 1
    )
    key_turned = norm_rotate(
        key_cols.reshape(tok_count, local_key_value_heads, CHANNEL_WIDTH),
        lookup_rms_gain,
        positions,
    )
    key_turned = key_turned.reshape(tok_count, local_key_value_heads * CHANNEL_WIDTH)
    query_grouped = query_turned.reshape(
        tok_count, local_key_value_heads, local_group_count, CHANNEL_WIDTH
    ).transpose(1, 2, 0, 3)
    inverse_root_width = (softness_per_channel / math.sqrt(CHANNEL_WIDTH)).reshape(
        local_key_value_heads, local_group_count, 1, 1
    )

    def absorb(run_state, key_span, value_span):
        run_max, run_sum, run_acc = run_state
        scores = (
            jnp.einsum(
                "kgqd,nkd->kgqn", query_grouped, key_span, preferred_element_type=jnp.float32
            )
            * inverse_root_width
        )
        new_max = jnp.maximum(run_max, jnp.max(scores, axis=-1))
        factor = jnp.exp(run_max - new_max)
        exp_terms = jnp.exp(scores - new_max[..., None])
        run_sum = run_sum * factor + jnp.sum(exp_terms, axis=-1)
        run_acc = run_acc * factor[..., None] + jnp.einsum(
            "kgqn,nkd->kgqd",
            exp_terms.astype(jnp.bfloat16),
            value_span,
            preferred_element_type=jnp.float32,
        )
        return (new_max, run_sum, run_acc)

    initial = (
        jnp.full((local_key_value_heads, local_group_count, tok_count), NEGATIVE, jnp.float32),
        jnp.zeros((local_key_value_heads, local_group_count, tok_count), jnp.float32),
        jnp.zeros(
            (local_key_value_heads, local_group_count, tok_count, CHANNEL_WIDTH), jnp.float32
        ),
    )
    key_piece = lax.all_gather(key_turned, "sp", axis=0, tiled=True)
    value_piece = lax.all_gather(value_cols, "sp", axis=0, tiled=True)
    piece_len = key_piece.shape[0]
    span_len = 1024
    span_count = piece_len // span_len
    key_spans = key_piece.reshape(span_count, span_len, local_key_value_heads, CHANNEL_WIDTH)
    value_spans = value_piece.reshape(span_count, span_len, local_key_value_heads, CHANNEL_WIDTH)

    def step_span(inner_state, span_pair):
        return (absorb(inner_state, span_pair[0], span_pair[1]), None)

    result_state, unused = lax.scan(step_span, initial, (key_spans, value_spans))
    final_max, final_sum, final_acc = result_state
    attn_heads = (final_acc / final_sum[..., None]).astype(jnp.bfloat16)
    attn_flat = attn_heads.transpose(2, 0, 1, 3).reshape(tok_count, heads_here * CHANNEL_WIDTH)
    partial_sum = jnp.dot(attn_flat, mixing_exit_weights, preferred_element_type=jnp.float32)
    share_width = model_width // lax.axis_size("tp")
    first_col = tp_position * share_width
    attended = lax.psum(partial_sum.astype(jnp.bfloat16), "tp")
    mid_rows = (skip_stream_input.astype(jnp.float32) + attended.astype(jnp.float32)).astype(
        jnp.bfloat16
    )
    mid_wide = mid_rows.astype(jnp.float32)
    normed_rows = (
        mid_wide
        * lax.rsqrt(jnp.mean(mid_wide * mid_wide, axis=-1, keepdims=True) + EPSILON)
        * specialist_rms_gain
    ).astype(jnp.bfloat16)
    mid_share = lax.dynamic_slice_in_dim(mid_rows, first_col, share_width, 1)
    outgoing_rows = lax.dynamic_slice_in_dim(normed_rows, first_col, share_width, 1)
    experts_count = lax.axis_size("sp")
    top_count = selected_specialist_ids.shape[1]
    capacity = max(2, 3 * tok_count * top_count // (2 * experts_count))
    flat_ids = selected_specialist_ids.reshape(-1)
    one_hot = (flat_ids[:, None] == jnp.arange(experts_count, dtype=jnp.int32)[None, :]).astype(
        jnp.int32
    )
    earlier = jnp.cumsum(one_hot, axis=0) - one_hot
    slot_index = jnp.sum(earlier * one_hot, axis=1)
    destination = flat_ids * capacity + slot_index
    owner_rows = jnp.arange(tok_count * top_count, dtype=jnp.int32) // top_count
    slot_owner = jnp.zeros((experts_count * capacity,), jnp.int32).at[destination].set(owner_rows)
    filled = jnp.zeros((experts_count * capacity,), jnp.int32).at[destination].set(1)
    outgoing = jnp.where(
        filled[:, None] > 0, outgoing_rows[slot_owner], jnp.zeros((), jnp.bfloat16)
    )
    outgoing = outgoing.reshape(experts_count, capacity, outgoing_rows.shape[1])
    gate_local = specialist_switch_weights[0]
    up_local = specialist_widen_weights[0]
    down_local = specialist_shrink_weights[0]
    arrived = lax.all_to_all(outgoing, "sp", split_axis=0, concat_axis=0, tiled=True)
    row_count = arrived.shape[0] * arrived.shape[1]
    feature_piece = lax.all_gather(arrived, "tp", axis=2, tiled=True)
    piece_width = feature_piece.shape[2]
    flat_piece = feature_piece.reshape(row_count, piece_width)
    gate_acc = jnp.dot(flat_piece, gate_local, preferred_element_type=jnp.float32)
    up_acc = jnp.dot(flat_piece, up_local, preferred_element_type=jnp.float32)
    hidden = (jax.nn.silu(gate_acc) * up_acc).astype(jnp.bfloat16)
    expert_part = jnp.dot(hidden, down_local, preferred_element_type=jnp.float32)
    expert_part = expert_part.reshape(arrived.shape[0], arrived.shape[1], model_width)
    expert_share = lax.psum_scatter(
        expert_part.astype(jnp.bfloat16), "tp", scatter_dimension=2, tiled=True
    )
    returned = lax.all_to_all(expert_share, "sp", split_axis=0, concat_axis=0, tiled=True)
    back_flat = returned.reshape(experts_count * capacity, share_width)
    picked = back_flat[destination].reshape(tok_count, top_count, share_width).astype(jnp.float32)
    route_weights = jax.nn.softmax(selected_dispatch_weights, axis=-1)
    layer_out = mid_share.astype(jnp.float32) + jnp.sum(route_weights[..., None] * picked, axis=1)
    return layer_out.astype(jnp.bfloat16)


def solution(mesh):
    in_specs = (
        P("sp", None),
        P("sp", "tp"),
        P("sp", None),
        P("sp", None),
        P(),
        P(),
        P("tp"),
        P("tp", None),
        P(),
        P("sp", None),
        P("sp", None),
        P("sp", None, "tp"),
        P("sp", None, "tp"),
        P("sp", "tp", None),
    )
    out_specs = P("sp", "tp")
    return jax.shard_map(shards, mesh=mesh, in_specs=in_specs, out_specs=out_specs, check_vma=False)
```

profile of v0, /device:TPU:0, one launch (start us, length us, event | category | flops | bytes accessed | tf_op | source)
XLA Modules:
  0.0 204.7 jit_solution(4723165117829957611)
XLA Ops:
  6.5 0.0 copy-start
  6.5 0.0 all-reduce.2.cloned.1.call-start
  6.6 0.9 constant_dynamic-slice_fusion.1
  7.5 0.1 copy.35
  7.7 0.7 fusion.35
  8.4 0.5 multiply_cosine_fusion.1
  9.0 0.2 fusion.55
  9.2 28.3 %all_gather.9 = bf16[1024,128]{0,1:T(8,128)(2,1)S(1)} all-gather(bf16[128,128]{0,1:T(8,128)(2,1)S(1)} %pad_maximum_fusion), channel_id=1, replica_groups=mesh['sp'=8,'tp'=4] {'sp'}, dimensions={0}, use_global_device_ids=true | all-gather | bytes 294912 | tf_op jit(solution)/shard_map/all_gather | solution.py:122
  37.5 1.0 copy.24
  38.6 0.1 copy.25
  38.7 0.7 broadcast_multiply_fusion.1
  39.4 0.8 multiply_multiply_fusion
  40.2 0.3 fusion.23
  40.5 0.6 multiply_reduce_fusion
  41.1 1.3 copy-done.1
  42.4 0.5 fusion.5
  42.9 0.8 constant_dynamic-slice_fusion
  43.7 0.1 copy.36
  43.8 0.0 copy-start.2
  43.8 26.8 %all_gather.10 = bf16[1024,128]{0,1:T(8,128)(2,1)S(1)} all-gather(bf16[128,128]{0,1:T(8,128)(2,1)S(1)} %copy.36), channel_id=1, replica_groups=mesh['sp'=8,'tp'=4] {'sp'}, dimensions={0}, use_global_device_ids=true | all-gather | bytes 294912 | tf_op jit(solution)/shard_map/all_gather | solution.py:123
  70.7 2.2 %fusion.14 = bf16[4,128,128]{1,2,0:T(8,128)(2,1)S(1)} fusion(f32[4,128,1024]{2,1,0:T(8,128)} %copy-done.1, f32[4,128]{1,0:T(4,128)S(1)} %broadcast_maximum_fusion, f32[4]{0:T(128)S(1)} %broadcast_multiply_fusion.1, bf16[1024,128]{0,1:T(8,128)(2,1)S(1)} %all_gather.10, f32[4,128]{1,0:T(4,128)S(1)} %get-tuple-element.44, f32[4,128]{1,0:T(4,128)S(1)} %get-tuple-element.43), kind=kOutput, calls=%fused_computation.19 | convolution fusion | flops 135987200 | bytes 2496528 | tf_op jit(solution)/shard_map/while/body/eval_jaxpr/kgqn,nkd->kgqd/dot_general | solution.py:107
  72.9 0.0 copy-start.5
  72.9 0.0 copy-start.3
  72.9 0.0 copy-done.2
  72.9 1.3 convolution_convert_fusion.1
  74.2 0.0 all-reduce.2.cloned.1.call-update
  74.2 0.0 all-gather.2.cloned.1.call-start
  74.3 0.0 copy-done.5
  74.3 0.1 copy.31
  74.4 0.1 eq.32
  74.5 0.1 eq.28
  74.7 0.6 reduce-window.6
  75.3 0.2 slice_reduce_fusion
  75.5 0.1 copy.30
  75.7 0.1 mul.356
  75.8 0.1 fusion.53
  75.9 1.4 scatter_custom_fusion.1
  77.3 1.4 scatter_custom_fusion
  78.7 0.1 broadcast_in_dim.23
  78.8 0.8 dynamic-slice
  79.6 25.8 %all-reduce.2.cloned.1.call-done = bf16[128,2048]{1,0:T(8,128)(2,1)} async-done(((bf16[128,2048]{1,0:T(8,128)(2,1)}), bf16[128,2048]{1,0:T(8,128)(2,1)}) %all-reduce.2.cloned.1.call-update) | async-done | bytes 524304 | tf_op jit(solution)/shard_map/psum | solution.py:140
  105.4 0.0 copy-done.3
  105.4 1.3 multiply_reduce_fusion.1
  106.7 0.1 convert_element_type.107
  106.8 0.1 fusion.19
  106.9 2.1 %gather_fusion = bf16[384,512]{1,0:T(8,128)(2,1)S(1)} fusion(bf16[128,512]{1,0:T(8,128)(2,1)S(1)} %fusion.19, s32[1024]{0:T(1024)S(1)} %pad_clamp_fusion.1), kind=kCustom, calls=%fused_computation | custom fusion | bytes 787968 | tf_op jit(solution)/shard_map/gather | solution.py:166
  109.0 0.1 broadcast_select_fusion
  109.1 16.5 %all_to_all.10 = bf16[8,48,512]{2,1,0:T(8,128)(2,1)} all-to-all(bf16[8,48,512]{2,1,0:T(8,128)(2,1)S(1)} %broadcast_select_fusion), channel_id=1, replica_groups=mesh['sp'=8,'tp'=4] {'sp'}, dimensions={0} | all-to-all | bytes 786432 | tf_op jit(solution)/shard_map/all_to_all | solution.py:172
  125.6 0.0 all-gather.2.cloned.1.call-update
  125.6 0.0 reduce-scatter.2.cloned.1.call-start
  125.7 18.0 %all-gather.2.cloned.1.call-done = bf16[8,48,2048]{2,1,0:T(8,128)(2,1)} async-done(((bf16[8,48,512]{2,1,0:T(8,128)(2,1)}), bf16[8,48,2048]{2,1,0:T(8,128)(2,1)}) %all-gather.2.cloned.1.call-update) | async-done | bytes 1572880 | tf_op jit(solution)/shard_map/all_gather | solution.py:174
  143.7 3.2 %fusion.3 = f32[384,512]{1,0:T(8,128)S(1)} fusion(bf16[384,2048]{1,0:T(8,128)(2,1)} %bitcast.82, bf16[1,2048,512]{2,1,0:T(8,128)(2,1)} %param.25), kind=kOutput, calls=%fused_computation.9 | convolution fusion | flops 805306368 | bytes 4456448 | tf_op jit(solution)/shard_map/dot_general | solution.py:177
  146.9 1.0 fusion.10
  147.9 2.1 %convolution_convert_fusion = bf16[8,48,2048]{2,1,0:T(8,128)(2,1)} fusion(bf16[8,48,512]{2,1,0:T(8,128)(2,1)S(1)} %bitcast.84, bf16[1,512,2048]{2,1,0:T(8,128)(2,1)S(1)} %copy-done), kind=kOutput, calls=%fused_computation.4 | convolution fusion | flops 806092800 | bytes 4063232 | tf_op jit(solution)/shard_map/dot_general | solution.py:180
  150.0 0.0 reduce-scatter.2.cloned.1.call-update
  150.1 28.1 %reduce-scatter.2.cloned.1.call-done = bf16[8,48,512]{2,1,0:T(8,128)(2,1)} async-done(((bf16[8,48,2048]{2,1,0:T(8,128)(2,1)}), bf16[8,48,512]{2,1,0:T(8,128)(2,1)}) %reduce-scatter.2.cloned.1.call-update) | async-done | bytes 393232 | tf_op jit(solution)/shard_map/reduce_scatter | solution.py:182
  178.2 5.5 %all-to-all-start.1 = ((bf16[8,48,512]{2,1,0:T(8,128)(2,1)}), bf16[8,48,512]{2,1,0:T(8,128)(2,1)S(1)}, u32[]{:S(2)}, u32[]{:S(2)}) async-start(bf16[8,48,512]{2,1,0:T(8,128)(2,1)} %reduce-scatter.2.cloned.1.call-done), calls=%async_computation.2 | async-start | bytes 786432 | tf_op jit(solution)/shard_map/all_to_all | solution.py:185
  183.7 0.0 copy-done.4
  183.8 0.1 copy.29
  183.9 11.4 %all-to-all-done.1 = bf16[8,48,512]{2,1,0:T(8,128)(2,1)S(1)} async-done(((bf16[8,48,512]{2,1,0:T(8,128)(2,1)}), bf16[8,48,512]{2,1,0:T(8,128)(2,1)S(1)}, u32[]{:S(2)}, u32[]{:S(2)}) %all-to-all-start.1) | async-done | bytes 393248 | tf_op jit(solution)/shard_map/all_to_all | solution.py:185
  195.3 1.2 gather_fusion.1
  196.4 0.3 reshape.493
  196.8 0.7 multiply_reduce_fusion.2
  197.5 0.7 add_convert_fusion.1
  (31 shorter events, 0.3 us)
Async XLA Ops:
  6.5 141.4 %copy-start = (bf16[1,512,2048]{2,1,0:T(8,128)(2,1)S(1)}, bf16[1,512,2048]{2,1,0:T(8,128)(2,1)}, u32[]{:S(2)}) copy-start(bf16[1,512,2048]{2,1,0:T(8,128)(2,1)} %param.27) | copy-start | bytes 6291460
  6.5 98.8 %all-reduce.2.cloned.1.call-start = ((), (), s32[]{:S(2)}) async-start(), calls=%async_computation.3 | async-start | bytes 1048576 | tf_op jit(solution)/shard_map/psum | solution.py:140
  41.1 1.4 copy-start.1
  43.8 29.1 %copy-start.2 = (bf16[512,2048]{1,0:T(8,128)(2,1)S(1)}, bf16[512,2048]{1,0:T(8,128)(2,1)}, u32[]{:S(2)}) copy-start(bf16[512,2048]{1,0:T(8,128)(2,1)} %param.21) | copy-start | bytes 6291460
  72.9 1.4 copy-start.5
  72.9 32.5 %copy-start.3 = (bf16[128,2048]{1,0:T(8,128)(2,1)S(1)}, bf16[128,2048]{1,0:T(8,128)(2,1)}, u32[]{:S(2)}) copy-start(bf16[128,2048]{1,0:T(8,128)(2,1)} %param.14) | copy-start | bytes 1572868
  74.2 69.4 %all-gather.2.cloned.1.call-start = ((), (), s32[]{:S(2)}) async-start(), calls=%async_computation.4 | async-start | bytes 1966080 | tf_op jit(solution)/shard_map/all_gather | solution.py:174
  125.6 52.6 %reduce-scatter.2.cloned.1.call-start = ((), (), s32[]{:S(2)}) async-start(), calls=%async_computation.5 | async-start | bytes 1966080 | tf_op jit(solution)/shard_map/reduce_scatter | solution.py:182
  143.7 3.2 %copy-start.6 = (bf16[1,2048,512]{2,1,0:T(8,128)(2,1)S(1)}, bf16[1,2048,512]{2,1,0:T(8,128)(2,1)}, u32[]{:S(2)}) copy-start(bf16[1,2048,512]{2,1,0:T(8,128)(2,1)} %param.26) | copy-start | bytes 6291460
  143.7 3.2 %copy-start.7 = (bf16[8,48,2048]{2,1,0:T(8,128)(2,1)S(1)}, bf16[8,48,2048]{2,1,0:T(8,128)(2,1)}, u32[]{:S(2)}) copy-start(bf16[8,48,2048]{2,1,0:T(8,128)(2,1)} %all-gather.2.cloned.1.call-done) | copy-start | bytes 4718596
  150.0 33.7 %copy-start.4 = (f32[128,2]{0,1:T(2,128)S(1)}, f32[128,2]{0,1:T(2,128)}, u32[]{:S(2)}) copy-start(f32[128,2]{0,1:T(2,128)} %param.23) | copy-start | bytes 3076
  178.2 17.1 %all-to-all-start.1 = ((bf16[8,48,512]{2,1,0:T(8,128)(2,1)}), bf16[8,48,512]{2,1,0:T(8,128)(2,1)S(1)}, u32[]{:S(2)}, u32[]{:S(2)}) async-start(bf16[8,48,512]{2,1,0:T(8,128)(2,1)} %reduce-scatter.2.cloned.1.call-done), calls=%async_computation.2 | async-start | bytes 786432 | tf_op jit(solution)/shard_map/all_to_all | solution.py:185
Sparse Core Ops, SparseCore 0:
  74.3 30.9 all-reduce.1
  125.8 17.8 all-gather.1
  150.2 27.9 reduce-scatter.1
where the time goes:
time: 205 us
  waiting for transfers between devices  83.3 us (41%)
  blocking collectives  71.7 us (35%)
  between operations  13.5 us (7%)
  local copies, waits for them, and re-layouts  12.6 us (6%)
  matrix products  10.4 us (5%)
  other arithmetic  7.66 us (4%)
  starting transfers between devices  5.57 us (3%)
    all_gather x1, blocking collectives, shards(): key_piece = lax.all_gather(key_turned, 'sp', axis=0, tiled=True)  28.3 us
    reduce_scatter x1, waiting for transfers between devices, shards(): lax.psum_scatter(expert_part.astype(jnp.bfloat16), 'tp', scatter_dimensio...  28.1 us
    all_gather x1, blocking collectives, shards(): value_piece = lax.all_gather(value_cols, 'sp', axis=0, tiled=True)  26.8 us
    psum x1, waiting for transfers between devices, shards(): attended = lax.psum(partial_sum.astype(jnp.bfloat16), 'tp')  25.8 us
    all_gather x1, waiting for transfers between devices, shards(): feature_piece = lax.all_gather(arrived, 'tp', axis=2, tiled=True)  18 us
    all_to_all x1, blocking collectives, shards(): lax.all_to_all(outgoing, 'sp', split_axis=0, concat_axis=0, tiled=True)  16.5 us
    all_to_all x1, waiting for transfers between devices, shards(): lax.all_to_all(expert_share, 'sp', split_axis=0, concat_axis=0, tiled=True)  11.4 us
    all_to_all x1, starting transfers between devices, shards(): lax.all_to_all(expert_share, 'sp', split_axis=0, concat_axis=0, tiled=True)  5.48 us
  transfers between devices with their start and end apart: 4, of which 4 were waited for; matrix products, arithmetic and copies ran while one was open for 3% of the time, Pallas kernels for 0%

commit v1 on v0

--- a/solution.py
+++ b/solution.py
@@ -171,7 +171,8 @@
     down_local = specialist_shrink_weights[0]
     arrived = lax.all_to_all(outgoing, "sp", split_axis=0, concat_axis=0, tiled=True)
     row_count = arrived.shape[0] * arrived.shape[1]
-    feature_piece = lax.all_gather(arrived, "tp", axis=2, tiled=True)
+    sent = jnp.stack([arrived] * lax.axis_size("tp"))
+    feature_piece = jnp.concatenate(lax.all_to_all(sent, "tp", 0, 0), axis=2)
     piece_width = feature_piece.shape[2]
     flat_piece = feature_piece.reshape(row_count, piece_width)
     gate_acc = jnp.dot(flat_piece, gate_local, preferred_element_type=jnp.float32)

time: 205 us -> 209 us (1.020)
  blocking collectives: 71.7 us -> 94.1 us
  waiting for transfers between devices: 83.3 us -> 63.1 us
  local copies, waits for them, and re-layouts: 12.6 us -> 16.2 us
  matrix products: 10.4 us -> 8.19 us
    all_to_all x0 -> x1, blocking collectives: none -> 22.5 us  [shards(): feature_piece = jnp.concatenate(lax.all_to_all(sent, 'tp', 0, 0), axis=2)]
    all_gather x1 -> x0, waiting for transfers between devices: 18 us -> none  [shards(): feature_piece = lax.all_gather(arrived, 'tp', axis=2, tiled=True)]
    reduce_scatter x1, waiting for transfers between devices: 28.1 us -> 25.9 us  [shards(): lax.psum_scatter(expert_part.astype(jnp.bfloat16), 'tp', scatter_dimensio...]
    dot_general x1, matrix products: 3.18 us -> 0.97 us  [shards(): jnp.dot(flat_piece, gate_local, preferred_element_type=jnp.float32)]
    unnamed x20 -> x21, local copies, waits for them, and re-layouts: 2.73 us -> 4.92 us
  transfers between devices with their start and end apart: 4 -> 3, of which waited for: 4 -> 3; matrix products, arithmetic and copies ran while one was open for 3% -> 3% of each run, Pallas kernels for 0% -> 0%
where the time goes in v1:
time: 209 us
  blocking collectives  94.1 us (45%)
  waiting for transfers between devices  63.1 us (30%)
  local copies, waits for them, and re-layouts  16.2 us (8%)
  between operations  13.8 us (7%)
  matrix products  8.19 us (4%)
  other arithmetic  7.66 us (4%)
  starting transfers between devices  5.57 us (3%)
    all_gather x1, blocking collectives, shards(): key_piece = lax.all_gather(key_turned, 'sp', axis=0, tiled=True)  28.3 us
    all_gather x1, blocking collectives, shards(): value_piece = lax.all_gather(value_cols, 'sp', axis=0, tiled=True)  26.8 us
    reduce_scatter x1, waiting for transfers between devices, shards(): lax.psum_scatter(expert_part.astype(jnp.bfloat16), 'tp', scatter_dimensio...  25.9 us
    psum x1, waiting for transfers between devices, shards(): attended = lax.psum(partial_sum.astype(jnp.bfloat16), 'tp')  25.8 us
    all_to_all x1, blocking collectives, shards(): feature_piece = jnp.concatenate(lax.all_to_all(sent, 'tp', 0, 0), axis=2)  22.5 us
    all_to_all x1, blocking collectives, shards(): lax.all_to_all(outgoing, 'sp', split_axis=0, concat_axis=0, tiled=True)  16.4 us
    all_to_all x1, waiting for transfers between devices, shards(): lax.all_to_all(expert_share, 'sp', split_axis=0, concat_axis=0, tiled=True)  11.4 us
    all_to_all x1, starting transfers between devices, shards(): lax.all_to_all(expert_share, 'sp', split_axis=0, concat_axis=0, tiled=True)  5.53 us
  transfers between devices with their start and end apart: 3, of which 3 were waited for; matrix products, arithmetic and copies ran while one was open for 3% of the time, Pallas kernels for 0%

profile of v1, /device:TPU:0, one launch (start us, length us, event | category | flops | bytes accessed | tf_op | source)
XLA Modules:
  0.0 208.5 jit_solution(7177825886643292036)
XLA Ops:
  6.5 0.0 copy-start
  6.5 0.0 all-reduce.2.cloned.1.call-start
  6.6 0.9 constant_dynamic-slice_fusion.1
  7.5 0.1 copy.44
  7.7 0.7 fusion.35
  8.4 0.5 multiply_cosine_fusion.1
  9.0 0.2 fusion.55
  9.2 28.3 %all_gather.6 = bf16[1024,128]{0,1:T(8,128)(2,1)S(1)} all-gather(bf16[128,128]{0,1:T(8,128)(2,1)S(1)} %pad_maximum_fusion), channel_id=1, replica_groups=mesh['sp'=8,'tp'=4] {'sp'}, dimensions={0}, use_global_device_ids=true | all-gather | bytes 294912 | tf_op jit(solution)/shard_map/all_gather | solution.py:122
  37.5 1.0 copy.32
  38.6 0.1 copy.33
  38.7 0.7 broadcast_multiply_fusion.1
  39.4 0.8 multiply_multiply_fusion
  40.2 0.3 fusion.23
  40.5 0.6 multiply_reduce_fusion
  41.1 1.3 copy-done.1
  42.4 0.5 fusion.5
  42.9 0.8 constant_dynamic-slice_fusion
  43.7 0.1 copy.45
  43.8 0.0 copy-start.2
  43.8 26.8 %all_gather.7 = bf16[1024,128]{0,1:T(8,128)(2,1)S(1)} all-gather(bf16[128,128]{0,1:T(8,128)(2,1)S(1)} %copy.45), channel_id=1, replica_groups=mesh['sp'=8,'tp'=4] {'sp'}, dimensions={0}, use_global_device_ids=true | all-gather | bytes 294912 | tf_op jit(solution)/shard_map/all_gather | solution.py:123
  70.7 2.2 %fusion.14 = bf16[4,128,128]{1,2,0:T(8,128)(2,1)S(1)} fusion(f32[4,128,1024]{2,1,0:T(8,128)} %copy-done.1, f32[4,128]{1,0:T(4,128)S(1)} %broadcast_maximum_fusion, f32[4]{0:T(128)S(1)} %broadcast_multiply_fusion.1, bf16[1024,128]{0,1:T(8,128)(2,1)S(1)} %all_gather.7, f32[4,128]{1,0:T(4,128)S(1)} %get-tuple-element.44, f32[4,128]{1,0:T(4,128)S(1)} %get-tuple-element.43), kind=kOutput, calls=%fused_computation.19 | convolution fusion | flops 135987200 | bytes 2496528 | tf_op jit(solution)/shard_map/while/body/eval_jaxpr/kgqn,nkd->kgqd/dot_general | solution.py:107
  72.9 0.0 copy-start.5
  72.9 0.0 copy-start.3
  72.9 1.3 convolution_convert_fusion.1
  74.2 0.0 all-reduce.2.cloned.1.call-update
  74.2 0.0 reduce-scatter.2.cloned.1.call-start
  74.3 0.1 copy.39
  74.4 0.1 eq.32
  74.5 0.1 eq.28
  74.7 0.6 reduce-window.6
  75.3 0.2 slice_reduce_fusion
  75.5 0.1 copy.38
  75.7 0.1 mul.356
  75.8 0.1 fusion.53
  75.9 1.4 scatter_custom_fusion.1
  77.3 1.4 scatter_custom_fusion
  78.7 0.1 broadcast_in_dim.23
  78.8 0.8 dynamic-slice
  79.6 25.8 %all-reduce.2.cloned.1.call-done = bf16[128,2048]{1,0:T(8,128)(2,1)} async-done(((bf16[128,2048]{1,0:T(8,128)(2,1)}), bf16[128,2048]{1,0:T(8,128)(2,1)}) %all-reduce.2.cloned.1.call-update) | async-done | bytes 524304 | tf_op jit(solution)/shard_map/psum | solution.py:140
  105.4 1.3 multiply_reduce_fusion.1
  106.7 0.1 convert_element_type.107
  106.8 0.1 fusion.19
  106.9 2.1 gather_fusion
  109.0 0.1 broadcast_select_fusion
  109.1 16.4 %all_to_all.15 = bf16[8,48,512]{2,1,0:T(8,128)(2,1)S(1)} all-to-all(bf16[8,48,512]{2,1,0:T(8,128)(2,1)S(1)} %broadcast_select_fusion), channel_id=1, replica_groups=mesh['sp'=8,'tp'=4] {'sp'}, dimensions={0} | all-to-all | bytes 786432 | tf_op jit(solution)/shard_map/all_to_all | solution.py:172
  125.5 0.2 stack.2
  125.7 22.5 %all_to_all.16 = bf16[4,8,48,512]{3,2,1,0:T(8,128)(2,1)S(1)} all-to-all(bf16[4,8,48,512]{3,2,1,0:T(8,128)(2,1)S(1)} %stack.2), channel_id=1, replica_groups=mesh['sp'=8,'tp'=4] {'tp'}, dimensions={0} | all-to-all | bytes 3145728 | tf_op jit(solution)/shard_map/all_to_all | solution.py:175
  148.2 1.2 copy.41
  149.4 0.0 copy-start.6
  149.4 0.4 copy.46
  149.9 1.1 copy-done.6
  151.0 1.0 fusion.3
  152.0 0.6 copy-done.7
  152.6 1.0 fusion.10
  153.6 2.1 %convolution_convert_fusion = bf16[8,48,2048]{2,1,0:T(8,128)(2,1)} fusion(bf16[8,48,512]{2,1,0:T(8,128)(2,1)S(1)} %bitcast.89, bf16[1,512,2048]{2,1,0:T(8,128)(2,1)S(1)} %copy-done), kind=kOutput, calls=%fused_computation.4 | convolution fusion | flops 806092800 | bytes 4063232 | tf_op jit(solution)/shard_map/dot_general | solution.py:181
  155.8 0.0 reduce-scatter.2.cloned.1.call-update
  155.8 25.9 %reduce-scatter.2.cloned.1.call-done = bf16[8,48,512]{2,1,0:T(8,128)(2,1)} async-done(((bf16[8,48,2048]{2,1,0:T(8,128)(2,1)}), bf16[8,48,512]{2,1,0:T(8,128)(2,1)}) %reduce-scatter.2.cloned.1.call-update) | async-done | bytes 393232 | tf_op jit(solution)/shard_map/reduce_scatter | solution.py:183
  181.7 5.5 %all-to-all-start.2 = ((bf16[8,48,512]{2,1,0:T(8,128)(2,1)}), bf16[8,48,512]{2,1,0:T(8,128)(2,1)S(1)}, u32[]{:S(2)}, u32[]{:S(2)}) async-start(bf16[8,48,512]{2,1,0:T(8,128)(2,1)} %reduce-scatter.2.cloned.1.call-done), calls=%async_computation.3 | async-start | bytes 786432 | tf_op jit(solution)/shard_map/all_to_all | solution.py:186
  187.3 0.1 copy.37
  187.4 11.4 %all-to-all-done.2 = bf16[8,48,512]{2,1,0:T(8,128)(2,1)S(1)} async-done(((bf16[8,48,512]{2,1,0:T(8,128)(2,1)}), bf16[8,48,512]{2,1,0:T(8,128)(2,1)S(1)}, u32[]{:S(2)}, u32[]{:S(2)}) %all-to-all-start.2) | async-done | bytes 393248 | tf_op jit(solution)/shard_map/all_to_all | solution.py:186
  198.8 1.2 gather_fusion.1
  199.9 0.3 reshape.495
  200.3 0.7 multiply_reduce_fusion.2
  201.0 0.7 add_convert_fusion.1
  (32 shorter events, 0.3 us)
Async XLA Ops:
  6.5 147.1 %copy-start = (bf16[1,512,2048]{2,1,0:T(8,128)(2,1)S(1)}, bf16[1,512,2048]{2,1,0:T(8,128)(2,1)}, u32[]{:S(2)}) copy-start(bf16[1,512,2048]{2,1,0:T(8,128)(2,1)} %param.27) | copy-start | bytes 6291460
  6.5 98.8 %all-reduce.2.cloned.1.call-start = ((), (), s32[]{:S(2)}) async-start(), calls=%async_computation.4 | async-start | bytes 1048576 | tf_op jit(solution)/shard_map/psum | solution.py:140
  41.1 1.4 copy-start.1
  43.8 29.1 %copy-start.2 = (bf16[512,2048]{1,0:T(8,128)(2,1)S(1)}, bf16[512,2048]{1,0:T(8,128)(2,1)}, u32[]{:S(2)}) copy-start(bf16[512,2048]{1,0:T(8,128)(2,1)} %param.21) | copy-start | bytes 6291460
  72.9 1.4 copy-start.5
  72.9 32.5 %copy-start.3 = (bf16[128,2048]{1,0:T(8,128)(2,1)S(1)}, bf16[128,2048]{1,0:T(8,128)(2,1)}, u32[]{:S(2)}) copy-start(bf16[128,2048]{1,0:T(8,128)(2,1)} %param.14) | copy-start | bytes 1572868
  74.2 107.5 %reduce-scatter.2.cloned.1.call-start = ((), (), s32[]{:S(2)}) async-start(), calls=%async_computation.5 | async-start | bytes 1966080 | tf_op jit(solution)/shard_map/reduce_scatter | solution.py:183
  149.4 1.6 copy-start.6
  151.0 1.6 copy-start.7
  155.8 31.5 %copy-start.4 = (f32[128,2]{0,1:T(2,128)S(1)}, f32[128,2]{0,1:T(2,128)}, u32[]{:S(2)}) copy-start(f32[128,2]{0,1:T(2,128)} %param.23) | copy-start | bytes 3076
  181.7 17.1 %all-to-all-start.2 = ((bf16[8,48,512]{2,1,0:T(8,128)(2,1)}), bf16[8,48,512]{2,1,0:T(8,128)(2,1)S(1)}, u32[]{:S(2)}, u32[]{:S(2)}) async-start(bf16[8,48,512]{2,1,0:T(8,128)(2,1)} %reduce-scatter.2.cloned.1.call-done), calls=%async_computation.3 | async-start | bytes 786432 | tf_op jit(solution)/shard_map/all_to_all | solution.py:186
Sparse Core Ops, SparseCore 0:
  74.3 30.9 all-reduce.1
  155.9 25.7 reduce-scatter.1
